TPU v7x, 32 devices: a whole 2x2x4 slice. The times are simulated.
32 devices in a mesh: sp: 8 (over z, x), tp: 4 (over y, core).
Axes of the slice: x: 2, y: 2, z: 4, core: 2. Of those that a mesh axis runs over, the one named last changes fastest.
Arguments:
- queries: bfloat16 [1024, 1024], P('sp', 'tp'), may hold values from -160 to 160
- keys: bfloat16 [1024, 256], P('sp', 'tp'), may hold values from -5 to 5
- values: bfloat16 [1024, 256], P('sp', 'tp'), may hold values from -6 to 6
- cum_gate: float32 [1024, 16], P('sp', 'tp'), as said below
- doc_ids: int32 [1024], P('sp'), may hold values from 0 to 7, never falling along the last dimension, each value on 1 to 640 neighbouring positions
- residual: bfloat16 [1024, 2048], P(('sp', 'tp')), may hold values from -6 to 6
- out_proj: bfloat16 [1024, 2048], replicated, may hold values from -0.1875 to 0.1875
- norm_gain: float32 [2048], replicated, may hold values from 0.1 to 1.9
- route_ids: int32 [1024, 2], P(('sp', 'tp')), may hold values from 0 to 7, all different within a row; in each aligned block of 32 rows (0 to 31, 32 to 63, ...) at most 16 rows name the same one
- route_weights: float32 [1024, 2], P(('sp', 'tp')), may hold values from 0.2 to 1
- expert_gate: bfloat16 [8, 2048, 1024], P('sp', None, 'tp'), may hold values from -0.125 to 0.125
- expert_up: bfloat16 [8, 2048, 1024], P('sp', None, 'tp'), may hold values from -0.125 to 0.125
- expert_down: bfloat16 [8, 1024, 2048], P('sp', 'tp'), may hold values from -0.1875 to 0.1875
Outputs:
- mixed: bfloat16 [1024, 2048], P(('sp', 'tp'))
Inputs may be any that keep to these rules, and one draw needn't show every extreme that they name: `route_ids`: within each aligned block of 32 rows no expert is named by more than 16 rows, and in every draw some block has an expert named by exactly 16 rows; the 2 experts of a row differ. `doc_ids`: never falling along positions; a document spans at most 640 positions, and one spans exactly that many. `cum_gate`: never rising along positions.
All inputs are finite; a program needn't handle non-finite values.
Results may differ from a plain program's by a relative error of at most 0.014.
Values may be sent and summed in bfloat16 or wider, within the bound.
A program may use at most 128 MiB of HBM per device.

v0:
```python
import jax
import jax.numpy as jnp
from jax import lax
from jax.sharding import PartitionSpec as P

D = 2048
HEAD_DIM = 64
TOP = 2
very_low = -1e30
norm_eps = 1e-06


def slot_ranks(picked_ids, experts):
    onehot = (picked_ids[..., None] == jnp.arange(experts, dtype=jnp.int32)).astype(jnp.int32)
    earlier = jnp.cumsum(onehot, axis=-2) - onehot
    return jnp.sum(earlier * onehot, axis=-1)


def local(
    queries,
    keys,
    values,
    cum_gate,
    doc_ids,
    residual,
    out_proj,
    norm_gain,
    route_ids,
    route_weights,
    expert_gate,
    expert_up,
    expert_down,
):
    own_tokens = queries.shape[0]
    head_count = queries.shape[1] // HEAD_DIM
    kv_count = keys.shape[1] // HEAD_DIM
    group_size = head_count // kv_count
    scale = HEAD_DIM ** (-0.5)
    own_start = lax.axis_index("sp") * own_tokens
    query_pos = own_start + jnp.arange(own_tokens, dtype=jnp.int32)
    query_heads = queries.reshape(own_tokens, kv_count, group_size, HEAD_DIM)
    query_gate = cum_gate.reshape(own_tokens, kv_count, group_size)
    gate_all, doc_all = (
        lax.all_gather(cum_gate, "sp", axis=0, tiled=True),
        lax.all_gather(doc_ids, "sp", axis=0, tiled=True),
    )

    def attend(state, key_block, value_block, first, block_len):
        gate_keys = lax.dynamic_slice_in_dim(gate_all, first, block_len, 0)
        doc_keys = lax.dynamic_slice_in_dim(doc_all, first, block_len, 0)
        key_heads = key_block.reshape(block_len, kv_count, HEAD_DIM)
        value_heads = value_block.reshape(block_len, kv_count, HEAD_DIM)
        scores = (
            jnp.einsum("tkgd,skd->tkgs", query_heads, key_heads, preferred_element_type=jnp.float32)
            * scale
        )
        scores = (
            scores
            + query_gate[..., None]
            - gate_keys.T.reshape(kv_count, group_size, block_len)[None]
        )
        key_pos = first + jnp.arange(block_len, dtype=jnp.int32)
        allowed = (key_pos[None, :] <= query_pos[:, None]) & (doc_keys[None, :] == doc_ids[:, None])
        allowed = allowed[:, None, None, :]
        scores = jnp.where(allowed, scores, very_low)
        top_old, total_old, summed_old = state
        top_new = jnp.maximum(top_old, jnp.max(scores, axis=-1))
        weights = jnp.where(allowed, jnp.exp(scores - top_new[..., None]), 0.0)
        fade = jnp.exp(top_old - top_new)
        total_new = total_old * fade + jnp.sum(weights, axis=-1)
        summed_new = summed_old * fade[..., None] + jnp.einsum(
            "tkgs,skd->tkgd",
            weights.astype(jnp.bfloat16),
            value_heads,
            preferred_element_type=jnp.float32,
        )
        return (top_new, total_new, summed_new)

    start_state = (
        jnp.full((own_tokens, kv_count, group_size), very_low, jnp.float32),
        jnp.zeros((own_tokens, kv_count, group_size), jnp.float32),
        jnp.zeros((own_tokens, kv_count, group_size, HEAD_DIM), jnp.float32),
    )
    key_piece = lax.all_gather(keys, "sp", axis=0, tiled=True)
    value_piece = lax.all_gather(values, "sp", axis=0, tiled=True)
    piece_len = key_piece.shape[0]
    block_len = min(piece_len, own_tokens)

    def one_block(index, inner):
        offset = index * block_len
        key_block = lax.dynamic_slice_in_dim(key_piece, offset, block_len, 0)
        value_block = lax.dynamic_slice_in_dim(value_piece, offset, block_len, 0)
        last_doc = lax.dynamic_index_in_dim(doc_all, offset + block_len - 1, 0, keepdims=False)
        needed = (offset <= own_start + own_tokens - 1) & (last_doc >= doc_ids[0])
        return lax.cond(
            needed,
            lambda carried: attend(carried, key_block, value_block, offset, block_len),
            lambda carried: carried,
            inner,
        )

    top, total, summed = lax.fori_loop(0, piece_len // block_len, one_block, start_state)
    attended = (
        (summed / total[..., None]).reshape(own_tokens, head_count * HEAD_DIM).astype(jnp.bfloat16)
    )
    sp_count = lax.axis_size("sp")
    rows_dev = residual.shape[0]
    plane_entries = lax.all_to_all(attended, "tp", split_axis=0, concat_axis=1, tiled=True)
    projected = jnp.dot(plane_entries, out_proj, preferred_element_type=jnp.float32)
    stream = (residual.astype(jnp.float32) + projected).astype(jnp.bfloat16)
    stream_f = stream.astype(jnp.float32)
    normed = stream_f * lax.rsqrt(jnp.mean(stream_f * stream_f, axis=1, keepdims=True) + norm_eps)
    normed = (normed * norm_gain[None, :]).astype(jnp.bfloat16)
    exp_dev = expert_gate.shape[0]
    experts = exp_dev * sp_count
    capacity = max(2, 2 * rows_dev * TOP // experts)
    own_flat = route_ids.reshape(-1)
    own_rank = slot_ranks(route_ids.reshape(1, rows_dev * TOP), experts)[0]
    own_dest = own_flat * capacity + own_rank
    row_of = jnp.arange(rows_dev * TOP, dtype=jnp.int32) // TOP
    outgoing = jnp.zeros((experts * capacity, D), jnp.bfloat16).at[own_dest].set(normed[row_of])
    arrived = lax.all_to_all(
        outgoing.reshape(experts, capacity, D), "sp", split_axis=0, concat_axis=1, tiled=True
    )
    arrived = arrived.reshape(exp_dev, sp_count, 1, capacity, D)
    piece = lax.all_gather(arrived, "tp", axis=2, tiled=True)
    gate = jnp.einsum("esncd,edf->esncf", piece, expert_gate, preferred_element_type=jnp.float32)
    upper = jnp.einsum("esncd,edf->esncf", piece, expert_up, preferred_element_type=jnp.float32)
    hidden = (jax.nn.silu(gate) * upper).astype(jnp.bfloat16)
    partial_value = jnp.einsum(
        "esncf,efd->esncd", hidden, expert_down, preferred_element_type=jnp.float32
    )
    expert_sums = lax.psum_scatter(
        partial_value.astype(jnp.bfloat16), "tp", scatter_dimension=2, tiled=True
    )
    expert_out = expert_sums.reshape(exp_dev, sp_count * capacity, D)
    returned = lax.all_to_all(expert_out, "sp", split_axis=1, concat_axis=0, tiled=True)
    selected = returned.reshape(experts * capacity, D)[own_dest]
    weighted = selected.astype(jnp.float32).reshape(rows_dev, TOP, D) * route_weights[..., None]
    return (stream_f + jnp.sum(weighted, axis=1)).astype(jnp.bfloat16)


def solution(mesh):
    in_specs = (
        P("sp", "tp"),
        P("sp", "tp"),
        P("sp", "tp"),
        P("sp", "tp"),
        P("sp"),
        P(("sp", "tp"), None),
        P(),
        P(),
        P(("sp", "tp"), None),
        P(("sp", "tp"), None),
        P("sp", None, "tp"),
        P("sp", None, "tp"),
        P("sp", "tp", None),
    )
    out_specs = P(("sp", "tp"), None)
    return jax.shard_map(local, mesh=mesh, in_specs=in_specs, out_specs=out_specs, check_vma=False)
```

profile of v0, /device:TPU:0, one launch (start us, length us, event | category | flops | bytes accessed | tf_op | source)
XLA Modules:
  0.0 280.7 jit_solution(1329913075445038006)
XLA Ops:
  6.5 28.3 %all_gather.16 = bf16[1024,64]{0,1:T(8,128)(2,1)S(1)} all-gather(bf16[128,64]{0,1:T(8,128)(2,1)} %param.18), channel_id=1, replica_groups=mesh['sp'=8,'tp'=4] {'sp'}, dimensions={0}, use_global_device_ids=true | all-gather | bytes 147456 | tf_op jit(solution)/shard_map/all_gather | solution.py:84
  34.8 26.4 %all_gather.18 = bf16[1024,64]{0,1:T(8,128)(2,1)S(1)} all-gather(bf16[128,64]{0,1:T(8,128)(2,1)} %param.19), channel_id=1, replica_groups=mesh['sp'=8,'tp'=4] {'sp'}, dimensions={0}, use_global_device_ids=true | all-gather | bytes 147456 | tf_op jit(solution)/shard_map/all_gather | solution.py:85
  61.2 0.9 copy.35
  62.2 26.3 %all_gather.17 = f32[1024,4]{0,1:T(4,128)S(1)} all-gather(f32[128,4]{0,1:T(4,128)} %param.20), channel_id=1, replica_groups=mesh['sp'=8,'tp'=4] {'sp'}, dimensions={0}, use_global_device_ids=true | all-gather | bytes 18432 | tf_op jit(solution)/shard_map/all_gather | solution.py:44
  88.4 16.5 %all-gather.1 = s32[8,1,128]{2,1,0:T(1,128)S(1)} all-gather(s32[1,1,128]{2,1,0:T(1,128)} %bitcast.128), channel_id=1, replica_groups=mesh['sp'=8,'tp'=4] {'sp'}, dimensions={0}, use_global_device_ids=true | all-gather | bytes 4608 | tf_op jit(solution)/shard_map/all_gather | solution.py:45
  105.0 18.1 %while.23 = (s32[]{:T(128)}, f32[128,1,4]{0,2,1:T(4,128)S(1)}, f32[128,1,4]{0,2,1:T(4,128)S(1)}, f32[128,1,4,64]{0,3,2,1:T(8,128)S(1)}, s32[]{:T(128)}, /*index=...) while((s32[]{:T(128)}, f32[128,1,4]{0,2,1:T(4,128)S(1)}, ...), condition=%wide.region_5.6_spmd.clone, body=%wide.region_0.5_spmd.clone.sunk | while | flops 17614608 | bytes 1258975 | solution.py:102
  105.0 0.7 dynamic_slice.68
  106.9 2.1 conditional.3
  107.1 0.8 compare_and_fusion
  107.8 0.9 fusion.47
  109.1 0.7 dynamic_slice.68
  115.1 0.7 dynamic_slice.68
  119.1 0.7 dynamic_slice.68
  123.3 0.8 convert_element_type.76
  124.1 3.3 %all-to-all-start = ((bf16[4,32,256]{2,1,0:T(8,128)(2,1)}), bf16[4,32,256]{2,1,0:T(8,128)(2,1)S(1)}, u32[]{:S(2)}, u32[]{:S(2)}) async-start(bf16[4,32,256]{2,1,0:T(8,128)(2,1)} %convert_element_type.76), calls=%async_computation | async-start | bytes 131072 | tf_op jit(solution)/shard_map/all_to_all | solution.py:108
  128.2 3.2 %all-to-all-done = bf16[4,32,256]{2,1,0:T(8,128)(2,1)S(1)} async-done(((bf16[4,32,256]{2,1,0:T(8,128)(2,1)}), bf16[4,32,256]{2,1,0:T(8,128)(2,1)S(1)}, u32[]{:S(2)}, u32[]{:S(2)}) %all-to-all-start) | async-done | bytes 65568 | tf_op jit(solution)/shard_map/all_to_all | solution.py:108
  131.5 3.1 %multiply_reduce_fusion.1 = (f32[32]{0:T(128)S(1)}, f32[32,2048]{1,0:T(8,128)S(1)}) fusion(bf16[32,1024]{1,0:T(8,128)(2,1)S(1)} %bitcast.124, bf16[1024,2048]{1,0:T(8,128)(2,1)} %param.23, bf16[32,2048]{1,0:T(8,128)(2,1)S(1)} %copy-done.1), kind=kOutput, calls=%fused_computation.58 | convolution fusion | flops 134610912 | bytes 4653184 | tf_op jit(solution)/shard_map/dot_general | solution.py:109
  134.7 2.0 scatter_custom_fusion
  136.7 25.9 %all_to_all.34 = bf16[8,16,2048]{2,1,0:T(8,128)(2,1)} all-to-all(bf16[8,16,2048]{2,1,0:T(8,128)(2,1)S(1)} %bitcast.121), channel_id=1, replica_groups=mesh['sp'=8,'tp'=4] {'sp'}, dimensions={0} | all-to-all | bytes 1048576 | tf_op jit(solution)/shard_map/all_to_all | solution.py:122
  162.7 20.8 %all-gather.4.cloned.1.call-done = bf16[8,64,2048]{2,1,0:T(8,128)(2,1)} async-done(((bf16[8,16,2048]{2,1,0:T(8,128)(2,1)}), bf16[8,64,2048]{2,1,0:T(8,128)(2,1)}) %all-gather.4.cloned.1.call-update) | async-done | bytes 2097168 | tf_op jit(solution)/shard_map/all_gather | solution.py:126
  183.5 2.3 fusion.30
  185.8 5.5 %fusion.24 = bf16[1,8,4,16,2048]{4,3,2,1,0:T(8,128)(2,1)} fusion(bf16[1,256,2048]{2,1,0:T(8,128)(2,1)S(1)} %copy-done, bf16[8,4,16,2048]{3,2,1,0:T(8,128)(2,1)} %bitcast.132, bf16[1,2048,256]{2,1,0:T(8,128)(2,1)} %param.28, f32[8,4,16,256]{3,2,1,0:T(8,128)S(1)} %fusion.30), kind=kOutput, calls=%fused_computation.36 | convolution fusion | flops 1075576832 | bytes 6815744 | tf_op jit(solution)/shard_map/esncf,efd->esncd/dot_general | solution.py:130
  192.5 50.3 %all-reduce.3.cloned.1.call-done = bf16[1,8,4,16,2048]{4,3,2,1,0:T(8,128)(2,1)} async-done(((bf16[1,8,4,16,2048]{4,3,2,1,0:T(8,128)(2,1)}), bf16[1,8,4,16,2048]{4,3,2,1,0:T(8,128)(2,1)}) %all-reduce.3.cloned.1.call-update) | async-done | bytes 2097168
  242.8 1.7 constant_dynamic-slice_fusion
  244.6 0.8 copy.53
  245.9 3.7 %reduce.9 = bf16[128,2048]{1,0:T(8,128)(2,1)S(1)} reduce(bf16[128,1,2048]{2,1,0:T(2,128)(2,1)S(1)} %bitcast.119, bf16[]{:T(256)} %broadcast.235), dimensions={1}, to_apply=%bitcast.111.reduce_sub_computation | reduce | bytes 1048578
  249.6 1.2 reshape.400
  250.8 5.5 %all-to-all-start.2 = ((bf16[8,2,16384]{2,1,0:T(2,128)(2,1)}), bf16[8,2,16384]{2,1,0:T(2,128)(2,1)S(1)}, u32[]{:S(2)}, u32[]{:S(2)}) async-start(bf16[8,2,16384]{2,1,0:T(2,128)(2,1)} %reshape.400), calls=%async_computation.2 | async-start | bytes 1048576 | tf_op jit(solution)/shard_map/all_to_all | solution.py:137
  256.4 14.2 %all-to-all-done.2 = bf16[8,2,16384]{2,1,0:T(2,128)(2,1)S(1)} async-done(((bf16[8,2,16384]{2,1,0:T(2,128)(2,1)}), bf16[8,2,16384]{2,1,0:T(2,128)(2,1)S(1)}, u32[]{:S(2)}, u32[]{:S(2)}) %all-to-all-start.2) | async-done | bytes 524320 | tf_op jit(solution)/shard_map/all_to_all | solution.py:137
  271.4 0.7 gather_fusion
  272.5 0.7 multiply_reduce_fusion
  273.2 0.7 add_convert_fusion
  (71 shorter events, 7.3 us)
Async XLA Ops:
  6.5 179.3 %copy-start = (bf16[1,256,2048]{2,1,0:T(8,128)(2,1)S(1)}, bf16[1,256,2048]{2,1,0:T(8,128)(2,1)}, u32[]{:S(2)}) copy-start(bf16[1,256,2048]{2,1,0:T(8,128)(2,1)} %param.29) | copy-start | bytes 3145732
  104.9 22.5 %copy-start.3 = (s32[32,2]{0,1:T(2,128)S(1)}, s32[32,2]{0,1:T(2,128)}, u32[]{:S(2)}) copy-start(s32[32,2]{0,1:T(2,128)} %param.25) | copy-start | bytes 772
  105.0 26.5 %copy-start.1 = (bf16[32,2048]{1,0:T(8,128)(2,1)S(1)}, bf16[32,2048]{1,0:T(8,128)(2,1)}, u32[]{:S(2)}) copy-start(bf16[32,2048]{1,0:T(8,128)(2,1)} %param.22) | copy-start | bytes 393220
  124.1 7.4 %all-to-all-start = ((bf16[4,32,256]{2,1,0:T(8,128)(2,1)}), bf16[4,32,256]{2,1,0:T(8,128)(2,1)S(1)}, u32[]{:S(2)}, u32[]{:S(2)}) async-start(bf16[4,32,256]{2,1,0:T(8,128)(2,1)} %convert_element_type.76), calls=%async_computation | async-start | bytes 131072 | tf_op jit(solution)/shard_map/all_to_all | solution.py:108
  127.4 56.1 %all-gather.4.cloned.1.call-start = ((), (), s32[]{:S(2)}) async-start(), calls=%async_computation.3 | async-start | bytes 2621440 | tf_op jit(solution)/shard_map/all_gather | solution.py:126
  131.5 3.2 %copy-start.2 = (f32[2048]{0:T(1024)S(1)}, f32[2048]{0:T(1024)}, u32[]{:S(2)}) copy-start(f32[2048]{0:T(1024)} %param.24) | copy-start | bytes 24580
  134.6 48.9 %copy-start.5 = (bf16[1,2048,256]{2,1,0:T(8,128)(2,1)S(1)}, bf16[1,2048,256]{2,1,0:T(8,128)(2,1)}, u32[]{:S(2)}) copy-start(bf16[1,2048,256]{2,1,0:T(8,128)(2,1)} %param.27) | copy-start | bytes 3145732
  162.7 80.2 %all-reduce.3.cloned.1.call-start = ((), (), s32[]{:S(2)}) async-start(), calls=%async_computation.4 | async-start | bytes 4194304
  191.3 0.7 copy-start.6
  245.4 10.9 %copy-start.4 = (f32[32,2]{0,1:T(2,128)S(1)}, f32[32,2]{0,1:T(2,128)}, u32[]{:S(2)}) copy-start(f32[32,2]{0,1:T(2,128)} %param.26) | copy-start | bytes 772
  250.8 19.8 %all-to-all-start.2 = ((bf16[8,2,16384]{2,1,0:T(2,128)(2,1)}), bf16[8,2,16384]{2,1,0:T(2,128)(2,1)S(1)}, u32[]{:S(2)}, u32[]{:S(2)}) async-start(bf16[8,2,16384]{2,1,0:T(2,128)(2,1)} %reshape.400), calls=%async_computation.2 | async-start | bytes 1048576 | tf_op jit(solution)/shard_map/all_to_all | solution.py:137
Sparse Core Ops, SparseCore 0:
  162.8 20.6 all-gather.3
  191.4 51.3 all-reduce.2
where the time goes:
time: 282 us; the launch traced here: 281 us
  blocking collectives  123 us (44%)
  waiting for transfers between devices  88.5 us (31%)
  local copies, waits for them, and re-layouts  17 us (6%)
  between operations  13.7 us (5%)
  matrix products  12 us (4%)
  loops' own time  10.9 us (4%)
  starting transfers between devices  8.88 us (3%)
  other arithmetic  6.46 us (2%)
    unnamed x3, waiting for transfers between devices  50.4 us
    all_gather x1, blocking collectives, local(): key_piece = lax.all_gather(keys, 'sp', axis=0, tiled=True)  28.3 us
    all_gather x1, blocking collectives, local(): value_piece = lax.all_gather(values, 'sp', axis=0, tiled=True)  26.4 us
    all_gather x1, blocking collectives, local(): lax.all_gather(cum_gate, 'sp', axis=0, tiled=True)  26.3 us
    all_to_all x1, blocking collectives, local(): lax.all_to_all(outgoing.reshape(experts, capacity, D), 'sp', split_axis=0...  25.9 us
    all_gather x1, waiting for transfers between devices, local(): piece = lax.all_gather(arrived, 'tp', axis=2, tiled=True)  20.8 us
    all_gather x1, blocking collectives, local(): lax.all_gather(doc_ids, 'sp', axis=0, tiled=True)  16.5 us
    all_to_all x1, waiting for transfers between devices, local(): lax.all_to_all(expert_out, 'sp', split_axis=1, concat_axis=0, tiled=True)  14.2 us
  transfers between devices with their start and end apart: 4, of which 4 were waited for; matrix products, arithmetic and copies ran while one was open for 1% of the time, Pallas kernels for 0%

commit v1 on v0

--- a/solution.py
+++ b/solution.py
@@ -134,7 +134,10 @@
         partial_value.astype(jnp.bfloat16), "tp", scatter_dimension=2, tiled=True
     )
     expert_out = expert_sums.reshape(exp_dev, sp_count * capacity, D)
-    returned = lax.all_to_all(expert_out, "sp", split_axis=1, concat_axis=0, tiled=True)
+    returned = jnp.concatenate(
+        lax.all_to_all(jnp.stack(jnp.split(expert_out, lax.axis_size("sp"), axis=1)), "sp", 0, 0),
+        axis=0,
+    )
     selected = returned.reshape(experts * capacity, D)[own_dest]
     weighted = selected.astype(jnp.float32).reshape(rows_dev, TOP, D) * route_weights[..., None]
     return (stream_f + jnp.sum(weighted, axis=1)).astype(jnp.bfloat16)

time: 282 us -> 278 us (0.986)
  other arithmetic: 6.46 us -> 2.75 us
    unnamed x1 -> x0, other arithmetic: 3.7 us -> none
    unnamed x23 -> x26, local copies, waits for them, and re-layouts: 6.6 us -> 8.49 us
where the time goes in v1:
time: 278 us
  blocking collectives  123 us (44%)
  waiting for transfers between devices  88.5 us (32%)
  local copies, waits for them, and re-layouts  18.2 us (7%)
  between operations  13.6 us (5%)
  matrix products  12 us (4%)
  loops' own time  10.3 us (4%)
  starting transfers between devices  8.88 us (3%)
    unnamed x3, waiting for transfers between devices  50.4 us
    all_gather x1, blocking collectives, local(): key_piece = lax.all_gather(keys, 'sp', axis=0, tiled=True)  28.3 us
    all_gather x1, blocking collectives, local(): value_piece = lax.all_gather(values, 'sp', axis=0, tiled=True)  26.4 us
    all_gather x1, blocking collectives, local(): lax.all_gather(cum_gate, 'sp', axis=0, tiled=True)  26.3 us
    all_to_all x1, blocking collectives, local(): lax.all_to_all(outgoing.reshape(experts, capacity, D), 'sp', split_axis=0...  25.9 us
    all_gather x1, waiting for transfers between devices, local(): piece = lax.all_gather(arrived, 'tp', axis=2, tiled=True)  20.8 us
    all_gather x1, blocking collectives, local(): lax.all_gather(doc_ids, 'sp', axis=0, tiled=True)  16.5 us
    all_to_all x1, waiting for transfers between devices, local(): lax.all_to_all(jnp.stack(jnp.split(expert_out, lax.axis_size('sp'), axis=...  14.2 us
  transfers between devices with their start and end apart: 4, of which 4 were waited for; matrix products, arithmetic and copies ran while one was open for 1% of the time, Pallas kernels for 0%

profile of v1, /device:TPU:0, one launch (start us, length us, event | category | flops | bytes accessed | tf_op | source)
XLA Modules:
  0.0 277.6 jit_solution(1128100446252790359)
XLA Ops:
  6.5 28.3 %all_gather.16 = bf16[1024,64]{0,1:T(8,128)(2,1)S(1)} all-gather(bf16[128,64]{0,1:T(8,128)(2,1)} %param.18), channel_id=1, replica_groups=mesh['sp'=8,'tp'=4] {'sp'}, dimensions={0}, use_global_device_ids=true | all-gather | bytes 147456 | tf_op jit(solution)/shard_map/all_gather | solution.py:84
  34.8 26.4 %all_gather.18 = bf16[1024,64]{0,1:T(8,128)(2,1)S(1)} all-gather(bf16[128,64]{0,1:T(8,128)(2,1)} %param.19), channel_id=1, replica_groups=mesh['sp'=8,'tp'=4] {'sp'}, dimensions={0}, use_global_device_ids=true | all-gather | bytes 147456 | tf_op jit(solution)/shard_map/all_gather | solution.py:85
  61.2 0.9 copy.41
  62.2 26.3 %all_gather.17 = f32[1024,4]{0,1:T(4,128)S(1)} all-gather(f32[128,4]{0,1:T(4,128)} %param.20), channel_id=1, replica_groups=mesh['sp'=8,'tp'=4] {'sp'}, dimensions={0}, use_global_device_ids=true | all-gather | bytes 18432 | tf_op jit(solution)/shard_map/all_gather | solution.py:44
  88.4 16.5 %all-gather.1 = s32[8,1,128]{2,1,0:T(1,128)S(1)} all-gather(s32[1,1,128]{2,1,0:T(1,128)} %bitcast.159), channel_id=1, replica_groups=mesh['sp'=8,'tp'=4] {'sp'}, dimensions={0}, use_global_device_ids=true | all-gather | bytes 4608 | tf_op jit(solution)/shard_map/all_gather | solution.py:45
  105.0 17.0 %while.23 = (s32[]{:T(128)}, f32[128,1,4]{0,2,1:T(4,128)S(1)}, f32[128,1,4]{0,2,1:T(4,128)S(1)}, f32[128,1,4,64]{0,3,2,1:T(8,128)S(1)}, s32[]{:T(128)}, /*index=...) while((s32[]{:T(128)}, f32[128,1,4]{0,2,1:T(4,128)S(1)}, ...), condition=%wide.region_5.6_spmd.clone, body=%wide.region_0.5_spmd.clone.sunk | while | flops 17614608 | bytes 1258975 | solution.py:102
  106.8 2.1 conditional.3
  106.9 0.8 compare_and_fusion
  107.7 0.9 fusion.55
  122.1 0.8 convert_element_type.76
  122.9 3.3 %all-to-all-start = ((bf16[4,32,256]{2,1,0:T(8,128)(2,1)}), bf16[4,32,256]{2,1,0:T(8,128)(2,1)S(1)}, u32[]{:S(2)}, u32[]{:S(2)}) async-start(bf16[4,32,256]{2,1,0:T(8,128)(2,1)} %convert_element_type.76), calls=%async_computation | async-start | bytes 131072 | tf_op jit(solution)/shard_map/all_to_all | solution.py:108
  127.1 3.2 %all-to-all-done = bf16[4,32,256]{2,1,0:T(8,128)(2,1)S(1)} async-done(((bf16[4,32,256]{2,1,0:T(8,128)(2,1)}), bf16[4,32,256]{2,1,0:T(8,128)(2,1)S(1)}, u32[]{:S(2)}, u32[]{:S(2)}) %all-to-all-start) | async-done | bytes 65568 | tf_op jit(solution)/shard_map/all_to_all | solution.py:108
  130.3 3.1 %multiply_reduce_fusion.1 = (f32[32]{0:T(128)S(1)}, f32[32,2048]{1,0:T(8,128)S(1)}) fusion(bf16[32,1024]{1,0:T(8,128)(2,1)S(1)} %bitcast.155, bf16[1024,2048]{1,0:T(8,128)(2,1)} %param.23, bf16[32,2048]{1,0:T(8,128)(2,1)S(1)} %copy-done.1), kind=kOutput, calls=%fused_computation.57 | convolution fusion | flops 134610912 | bytes 4653184 | tf_op jit(solution)/shard_map/dot_general | solution.py:109
  133.6 2.0 scatter_custom_fusion
  135.6 25.9 %all_to_all.30 = bf16[8,16,2048]{2,1,0:T(8,128)(2,1)} all-to-all(bf16[8,16,2048]{2,1,0:T(8,128)(2,1)S(1)} %bitcast.152), channel_id=1, replica_groups=mesh['sp'=8,'tp'=4] {'sp'}, dimensions={0} | all-to-all | bytes 1048576 | tf_op jit(solution)/shard_map/all_to_all | solution.py:122
  161.6 20.8 %all-gather.4.cloned.1.call-done = bf16[8,64,2048]{2,1,0:T(8,128)(2,1)} async-done(((bf16[8,16,2048]{2,1,0:T(8,128)(2,1)}), bf16[8,64,2048]{2,1,0:T(8,128)(2,1)}) %all-gather.4.cloned.1.call-update) | async-done | bytes 2097168 | tf_op jit(solution)/shard_map/all_gather | solution.py:126
  182.4 2.3 fusion.30
  184.7 5.5 %fusion.24 = bf16[1,8,4,16,2048]{4,3,2,1,0:T(8,128)(2,1)} fusion(bf16[1,256,2048]{2,1,0:T(8,128)(2,1)S(1)} %copy-done, bf16[8,4,16,2048]{3,2,1,0:T(8,128)(2,1)} %bitcast.163, bf16[1,2048,256]{2,1,0:T(8,128)(2,1)} %param.28, f32[8,4,16,256]{3,2,1,0:T(8,128)S(1)} %fusion.30), kind=kOutput, calls=%fused_computation.36 | convolution fusion | flops 1075576832 | bytes 6815744 | tf_op jit(solution)/shard_map/esncf,efd->esncd/dot_general | solution.py:130
  191.4 50.3 %all-reduce.3.cloned.1.call-done = bf16[1,8,4,16,2048]{4,3,2,1,0:T(8,128)(2,1)} async-done(((bf16[1,8,4,16,2048]{4,3,2,1,0:T(8,128)(2,1)}), bf16[1,8,4,16,2048]{4,3,2,1,0:T(8,128)(2,1)}) %all-reduce.3.cloned.1.call-update) | async-done | bytes 2097168
  241.7 1.7 constant_dynamic-slice_fusion
  244.1 0.6 fusion.49
  244.7 0.6 fusion.48
  245.3 0.6 fusion.47
  245.9 0.6 fusion.46
  246.6 0.6 fusion.45
  247.2 0.6 fusion.44
  247.8 0.6 fusion.43
  248.5 5.5 %all-to-all-start.2 = ((bf16[8,1,16,2048]{3,2,1,0:T(8,128)(2,1)}), bf16[8,1,16,2048]{3,2,1,0:T(8,128)(2,1)S(1)}, u32[]{:S(2)}, u32[]{:S(2)}) async-start(bf16[8,1,16,2048]{3,2,1,0:T(8,128)(2,1)} %fusion.43), calls=%async_computation.2 | async-start | bytes 1048576 | tf_op jit(solution)/shard_map/all_to_all | solution.py:138
  254.1 14.2 %all-to-all-done.2 = bf16[8,1,16,2048]{3,2,1,0:T(8,128)(2,1)S(1)} async-done(((bf16[8,1,16,2048]{3,2,1,0:T(8,128)(2,1)}), bf16[8,1,16,2048]{3,2,1,0:T(8,128)(2,1)S(1)}, u32[]{:S(2)}, u32[]{:S(2)}) %all-to-all-start.2) | async-done | bytes 524320 | tf_op jit(solution)/shard_map/all_to_all | solution.py:138
  268.2 0.7 gather_fusion
  269.3 0.7 multiply_reduce_fusion
  270.1 0.7 add_convert_fusion
  (73 shorter events, 8.6 us)
Async XLA Ops:
  6.5 178.1 %copy-start = (bf16[1,256,2048]{2,1,0:T(8,128)(2,1)S(1)}, bf16[1,256,2048]{2,1,0:T(8,128)(2,1)}, u32[]{:S(2)}) copy-start(bf16[1,256,2048]{2,1,0:T(8,128)(2,1)} %param.29) | copy-start | bytes 3145732
  104.9 21.3 %copy-start.3 = (s32[32,2]{0,1:T(2,128)S(1)}, s32[32,2]{0,1:T(2,128)}, u32[]{:S(2)}) copy-start(s32[32,2]{0,1:T(2,128)} %param.25) | copy-start | bytes 772
  105.0 25.4 %copy-start.1 = (bf16[32,2048]{1,0:T(8,128)(2,1)S(1)}, bf16[32,2048]{1,0:T(8,128)(2,1)}, u32[]{:S(2)}) copy-start(bf16[32,2048]{1,0:T(8,128)(2,1)} %param.22) | copy-start | bytes 393220
  122.9 7.4 %all-to-all-start = ((bf16[4,32,256]{2,1,0:T(8,128)(2,1)}), bf16[4,32,256]{2,1,0:T(8,128)(2,1)S(1)}, u32[]{:S(2)}, u32[]{:S(2)}) async-start(bf16[4,32,256]{2,1,0:T(8,128)(2,1)} %convert_element_type.76), calls=%async_computation | async-start | bytes 131072 | tf_op jit(solution)/shard_map/all_to_all | solution.py:108
  126.2 56.1 %all-gather.4.cloned.1.call-start = ((), (), s32[]{:S(2)}) async-start(), calls=%async_computation.3 | async-start | bytes 2621440 | tf_op jit(solution)/shard_map/all_gather | solution.py:126
  130.3 3.2 %copy-start.2 = (f32[2048]{0:T(1024)S(1)}, f32[2048]{0:T(1024)}, u32[]{:S(2)}) copy-start(f32[2048]{0:T(1024)} %param.24) | copy-start | bytes 24580
  133.5 48.9 %copy-start.5 = (bf16[1,2048,256]{2,1,0:T(8,128)(2,1)S(1)}, bf16[1,2048,256]{2,1,0:T(8,128)(2,1)}, u32[]{:S(2)}) copy-start(bf16[1,2048,256]{2,1,0:T(8,128)(2,1)} %param.27) | copy-start | bytes 3145732
  161.5 80.2 %all-reduce.3.cloned.1.call-start = ((), (), s32[]{:S(2)}) async-start(), calls=%async_computation.4 | async-start | bytes 4194304
  190.1 0.7 copy-start.6
  190.2 63.8 %copy-start.4 = (f32[32,2]{0,1:T(2,128)S(1)}, f32[32,2]{0,1:T(2,128)}, u32[]{:S(2)}) copy-start(f32[32,2]{0,1:T(2,128)} %param.26) | copy-start | bytes 772
  248.5 19.8 %all-to-all-start.2 = ((bf16[8,1,16,2048]{3,2,1,0:T(8,128)(2,1)}), bf16[8,1,16,2048]{3,2,1,0:T(8,128)(2,1)S(1)}, u32[]{:S(2)}, u32[]{:S(2)}) async-start(bf16[8,1,16,2048]{3,2,1,0:T(8,128)(2,1)} %fusion.43), calls=%async_computation.2 | async-start | bytes 1048576 | tf_op jit(solution)/shard_map/all_to_all | solution.py:138
Sparse Core Ops, SparseCore 0:
  161.6 20.6 all-gather.3
  190.3 51.3 all-reduce.2
